TPU v7x, 32 devices: a whole 2x2x4 slice. The times are simulated.
32 devices in a mesh: fs: 8 (over z, x), tp: 4 (over y, core).
Axes of the slice: x: 2, y: 2, z: 4, core: 2. Of those that a mesh axis runs over, the one named last changes fastest.
Arguments:
- mixer_input: bfloat16 [8192, 4096], P('fs'), may hold values from -6 to 6
- cell_output: bfloat16 [8192, 2048], P('fs'), may hold values from -6 to 6
- query_grad: bfloat16 [8192, 2048], P('fs', 'tp'), may hold values from -4 to 4
- value_grad: bfloat16 [8192, 2048], P('fs', 'tp'), may hold values from -4 to 4
- output_grad: bfloat16 [8192, 4096], P('fs', 'tp'), may hold values from -4 to 4
- query_weight: float32 [4096, 2048], P('fs', 'tp'), may hold values from -6 to 6
- value_weight: float32 [4096, 2048], P('fs', 'tp'), may hold values from -6 to 6
- output_weight: float32 [2048, 4096], P('fs', 'tp'), may hold values from -6 to 6
- query_basis: bfloat16 [4096, 128], P('fs'), may hold values from -0.09375 to 0.09375
- value_basis: bfloat16 [4096, 128], P('fs'), may hold values from -0.09375 to 0.09375
- output_basis: bfloat16 [2048, 128], P('fs'), may hold values from -0.125 to 0.125
- query_mean: float32 [128, 2048], P(None, 'tp'), may hold values from -6 to 6
- value_mean: float32 [128, 2048], P(None, 'tp'), may hold values from -6 to 6
- output_mean: float32 [128, 4096], P(None, 'tp'), may hold values from -6 to 6
- query_square: float32 [128, 2048], P(None, 'tp'), may hold values from 0.25 to 4
- value_square: float32 [128, 2048], P(None, 'tp'), may hold values from 0.25 to 4
- output_square: float32 [128, 4096], P(None, 'tp'), may hold values from 0.25 to 4
Outputs:
- query_step: float32 [4096, 2048], P('fs', 'tp')
- value_step: float32 [4096, 2048], P('fs', 'tp')
- output_step: float32 [2048, 4096], P('fs', 'tp')
- query_copy: bfloat16 [4096, 2048], P(None, 'tp')
- value_copy: bfloat16 [4096, 2048], P(None, 'tp')
- output_copy: bfloat16 [2048, 4096], P(None, 'tp')
- query_first: float32 [128, 2048], P(None, 'tp')
- value_first: float32 [128, 2048], P(None, 'tp')
- output_first: float32 [128, 4096], P(None, 'tp')
- query_second: float32 [128, 2048], P(None, 'tp')
- value_second: float32 [128, 2048], P(None, 'tp')
- output_second: float32 [128, 4096], P(None, 'tp')
All inputs are finite; a program needn't handle non-finite values.
Results may differ from a plain program's by a relative error of at most 0.013.
Values may be sent and summed in bfloat16 or wider, within the bound.
No kernel may reach another device: no remote copies, remote signals or barrier semaphores. Data moves between devices by JAX's collectives and lax.ppermute only.
A program may use at most 128 MiB of HBM per device.

v0:
```python
import jax
import jax.numpy as jnp
from jax import lax
from jax.sharding import PartitionSpec as P

MODEL = 4096
CELL = 2048


beta_first = 0.8
beta_second = 0.9
floor_mean = 0.005
learn_rate = 0.05


def across(leading, trailing):
    return lax.dot_general(
        leading, trailing, (((0,), (0,)), ((), ())), preferred_element_type=jnp.float32
    )


def across_exact(leading, trailing):
    return lax.dot_general(
        leading,
        trailing,
        (((0,), (0,)), ((), ())),
        precision=lax.Precision.HIGHEST,
        preferred_element_type=jnp.float32,
    )


def product_exact(leading, trailing):
    return jnp.dot(
        leading, trailing, precision=lax.Precision.HIGHEST, preferred_element_type=jnp.float32
    )


def moments(projected, mean_old, square_old):
    moment_one = beta_first * mean_old + (1.0 - beta_first) * projected
    moment_two = beta_second * square_old + (1.0 - beta_second) * projected * projected
    return (moment_one, moment_two, moment_one / jnp.sqrt(moment_two))


def local(
    mixer_input,
    cell_output,
    query_grad,
    value_grad,
    output_grad,
    query_weight,
    value_weight,
    output_weight,
    query_basis,
    value_basis,
    output_basis,
    query_mean,
    value_mean,
    output_mean,
    query_square,
    value_square,
    output_square,
):
    local_query = query_basis.astype(jnp.float32)
    local_value = value_basis.astype(jnp.float32)
    local_output = output_basis.astype(jnp.float32)
    window = mixer_input
    first_sum = across_exact(
        lax.all_gather(query_basis, "fs", axis=0, tiled=True).astype(jnp.float32),
        across(window, query_grad),
    )
    second_sum = across_exact(
        lax.all_gather(value_basis, "fs", axis=0, tiled=True).astype(jnp.float32),
        across(window, value_grad),
    )
    window = cell_output
    part_output = across_exact(
        lax.all_gather(output_basis, "fs", axis=0, tiled=True).astype(jnp.float32),
        across(window, output_grad),
    )
    proj_query, proj_value, proj_output = lax.psum((first_sum, second_sum, part_output), "fs")
    query_first, query_second, query_dir = moments(proj_query, query_mean, query_square)
    value_first, value_second, value_dir = moments(proj_value, value_mean, value_square)
    output_first, output_second, output_dir = moments(proj_output, output_mean, output_square)
    low_query = product_exact(local_query, query_dir)
    low_value = product_exact(local_value, value_dir)
    low_output = product_exact(local_output, output_dir)
    partial_squares = (
        jnp.sum(low_query * low_query)
        + jnp.sum(low_value * low_value)
        + jnp.sum(low_output * low_output)
    )
    squares = lax.psum(partial_squares, ("fs", "tp"))
    factor = 1.0 / jnp.sqrt(squares / (3.0 * MODEL * CELL) + floor_mean)
    query_step = -factor * low_query
    value_step = -factor * low_value
    output_step = -factor * low_output
    query_copy, value_copy, output_copy = (
        lax.all_gather(
            (query_weight + learn_rate * query_step).astype(jnp.bfloat16), "fs", axis=0, tiled=True
        ),
        lax.all_gather(
            (value_weight + learn_rate * value_step).astype(jnp.bfloat16), "fs", axis=0, tiled=True
        ),
        lax.all_gather(
            (output_weight + learn_rate * output_step).astype(jnp.bfloat16),
            "fs",
            axis=0,
            tiled=True,
        ),
    )
    return (
        query_step,
        value_step,
        output_step,
        query_copy,
        value_copy,
        output_copy,
        query_first,
        value_first,
        output_first,
        query_second,
        value_second,
        output_second,
    )


def solution(mesh):
    in_specs = (
        P("fs", None),
        P("fs", None),
        P("fs", "tp"),
        P("fs", "tp"),
        P("fs", "tp"),
        P("fs", "tp"),
        P("fs", "tp"),
        P("fs", "tp"),
        P("fs", None),
        P("fs", None),
        P("fs", None),
        P(None, "tp"),
        P(None, "tp"),
        P(None, "tp"),
        P(None, "tp"),
        P(None, "tp"),
        P(None, "tp"),
    )
    out_specs = (
        P("fs", "tp"),
        P("fs", "tp"),
        P("fs", "tp"),
        P(None, "tp"),
        P(None, "tp"),
        P(None, "tp"),
        P(None, "tp"),
        P(None, "tp"),
        P(None, "tp"),
        P(None, "tp"),
        P(None, "tp"),
        P(None, "tp"),
    )
    return jax.shard_map(local, mesh=mesh, in_specs=in_specs, out_specs=out_specs, check_vma=False)
```

profile of v0, /device:TPU:0, one launch (start us, length us, event | category | flops | bytes accessed | tf_op | source)
XLA Modules:
  0.0 476.9 jit_solution(3303046204286626281)
XLA Ops:
  8.7 33.7 %all_gather.20 = bf16[2048,128]{1,0:T(8,128)(2,1)S(1)} all-gather(bf16[256,128]{1,0:T(8,128)(2,1)} %param.27), channel_id=1, replica_groups=mesh['fs'=8,'tp'=4] {'fs'}, dimensions={0}, use_global_device_ids=true | all-gather | bytes 589824 | tf_op jit(solution)/shard_map/all_gather | solution.py:77
  42.4 6.5 %fusion.14 = f32[2048,1024]{1,0:T(8,128)S(1)} fusion(bf16[1024,2048]{1,0:T(8,128)(2,1)} %param.18, bf16[1024,1024]{1,0:T(8,128)(2,1)S(1)} %copy-done), kind=kOutput, calls=%fused_computation.32 | convolution fusion | flops 4294967296 | bytes 14680064 | tf_op jit(solution)/shard_map/dot_general | solution.py:17
  49.0 7.5 %convolution_bitcast_fusion = f32[128,1024]{0,1:T(8,128)} fusion(f32[2048,1024]{1,0:T(8,128)S(1)} %fusion.14, bf16[2048,128]{1,0:T(8,128)(2,1)S(1)} %all_gather.20), kind=kOutput, calls=%fused_computation | convolution fusion | flops 3221225472 | bytes 9437184 | tf_op jit(solution)/shard_map/dot_general | solution.py:23
  56.5 6.7 %fusion.12 = f32[4096,512]{1,0:T(8,128)} fusion(bf16[1024,4096]{1,0:T(8,128)(2,1)S(1)} %bitcast.31, bf16[1024,512]{1,0:T(8,128)(2,1)S(1)} %copy-done.15), kind=kOutput, calls=%fused_computation.30 | convolution fusion | flops 4294967296 | bytes 17825792 | tf_op jit(solution)/shard_map/dot_general | solution.py:17
  63.2 6.8 %fusion.13 = f32[4096,512]{1,0:T(8,128)} fusion(bf16[1024,4096]{1,0:T(8,128)(2,1)S(1)} %bitcast.31, bf16[1024,512]{1,0:T(8,128)(2,1)S(1)} %copy-done.16), kind=kOutput, calls=%fused_computation.31 | convolution fusion | flops 4294967296 | bytes 17825792 | tf_op jit(solution)/shard_map/dot_general | solution.py:17
  70.0 11.1 %convolution_bitcast_fusion.2 = f32[128,512]{0,1:T(8,128)} fusion(f32[4096,512]{1,0:T(8,128)} %fusion.12, bf16[4096,128]{1,0:T(8,128)(2,1)} %all-gather.6.cloned.1.call-done), kind=kOutput, calls=%fused_computation.2 | convolution fusion | flops 3221225472 | bytes 9699328 | tf_op jit(solution)/shard_map/dot_general | solution.py:23
  81.1 13.9 %all-gather.8.cloned.1.call-done = bf16[4096,128]{1,0:T(8,128)(2,1)} async-done(((bf16[512,128]{1,0:T(8,128)(2,1)}), bf16[4096,128]{1,0:T(8,128)(2,1)}) %all-gather.8.cloned.1.call-update) | async-done | bytes 1048592 | tf_op jit(solution)/shard_map/all_gather | solution.py:72
  95.1 11.2 %convolution_bitcast_fusion.1 = f32[128,512]{0,1:T(8,128)} fusion(f32[4096,512]{1,0:T(8,128)} %fusion.13, bf16[4096,128]{1,0:T(8,128)(2,1)} %all-gather.8.cloned.1.call-done), kind=kOutput, calls=%fused_computation.1 | convolution fusion | flops 3221225472 | bytes 9699328 | tf_op jit(solution)/shard_map/dot_general | solution.py:23
  107.3 76.3 %all-reduce.3.cloned.1.call-done = (f32[128,512]{0,1:T(8,128)}, f32[128,512]{0,1:T(8,128)}, f32[128,1024]{0,1:T(8,128)}) async-done(((f32[128,512]{0,1:T(8,128)}, f32[128,512]{0,1:T(8,128)}, f32[128,1024]{0,1:T(8,128)}), (f32[128,512]{0,1:T(8,128)}, f32[128,512]{0,1:T(8,128)}, f32[128,1024]{0,1:T(8,128)})) %all-reduce.3.cloned.1.call-update) | async-done | bytes 1048592 | tf_op jit(solution)/shard_map/psum | solution.py:80
  189.4 2.2 multiply_reduce_fusion.2
  193.6 2.5 copy.36
  196.1 39.8 %psum.31 = f32[]{:T(128)} all-reduce(f32[]{:T(128)S(6)} %add.51), channel_id=1, replica_groups=mesh['fs'=8,'tp'=4] {'fs','tp'}, use_global_device_ids=true, to_apply=%region_6.0 | all-reduce | flops 1 | bytes 8 | tf_op jit(solution)/shard_map/psum | solution.py:92
  236.6 2.9 add_convert_fusion.1
  239.6 2.5 copy.37
  242.1 2.6 add_convert_fusion
  244.8 2.7 copy.35
  247.4 2.7 add_convert_fusion.2
  259.7 2.5 copy.40
  263.6 50.0 %all-gather.12.cloned.1.call-done = bf16[4096,512]{0,1:T(8,128)(2,1)} async-done(((bf16[512,512]{0,1:T(8,128)(2,1)}), bf16[4096,512]{0,1:T(8,128)(2,1)}) %all-gather.12.cloned.1.call-update) | async-done | bytes 4194320 | tf_op jit(solution)/shard_map/all_gather | solution.py:101
  313.6 6.5 %copy.42 = bf16[4096,512]{1,0:T(8,128)(2,1)} copy(bf16[4096,512]{0,1:T(8,128)(2,1)} %all-gather.12.cloned.1.call-done) | data formatting | bytes 8388608
  320.1 68.2 %all-gather.14.cloned.1.call-done = bf16[2048,1024]{0,1:T(8,128)(2,1)} async-done(((bf16[256,1024]{0,1:T(8,128)(2,1)}), bf16[2048,1024]{0,1:T(8,128)(2,1)}) %all-gather.14.cloned.1.call-update) | async-done | bytes 4194320 | tf_op jit(solution)/shard_map/all_gather | solution.py:104
  388.3 6.4 %copy.43 = bf16[2048,1024]{1,0:T(8,128)(2,1)} copy(bf16[2048,1024]{0,1:T(8,128)(2,1)} %all-gather.14.cloned.1.call-done) | data formatting | bytes 8388608
  394.7 68.9 %all-gather.10.cloned.1.call-done = bf16[4096,512]{0,1:T(8,128)(2,1)} async-done(((bf16[512,512]{0,1:T(8,128)(2,1)}), bf16[4096,512]{0,1:T(8,128)(2,1)}) %all-gather.10.cloned.1.call-update) | async-done | bytes 4194320 | tf_op jit(solution)/shard_map/all_gather | solution.py:98
  463.7 6.4 %copy.41 = bf16[4096,512]{1,0:T(8,128)(2,1)} copy(bf16[4096,512]{0,1:T(8,128)(2,1)} %all-gather.10.cloned.1.call-done) | data formatting | bytes 8388608
  (70 shorter events, 19.2 us)
Async XLA Ops:
  7.2 35.2 %copy-start = (bf16[1024,1024]{1,0:T(8,128)(2,1)S(1)}, bf16[1024,1024]{1,0:T(8,128)(2,1)}, u32[]{:S(2)}) copy-start(bf16[1024,1024]{1,0:T(8,128)(2,1)} %param.21) | copy-start | bytes 6291460
  7.2 62.8 %all-gather.6.cloned.1.call-start = ((), (), s32[]{:S(2)}) async-start(), calls=%async_computation | async-start | bytes 1179648 | tf_op jit(solution)/shard_map/all_gather | solution.py:68
  7.9 87.1 %all-gather.8.cloned.1.call-start = ((), (), s32[]{:S(2)}) async-start(), calls=%async_computation.1 | async-start | bytes 1179648 | tf_op jit(solution)/shard_map/all_gather | solution.py:72
  8.7 175.0 %all-reduce.3.cloned.1.call-start = ((), (), s32[]{:S(2)}) async-start(), calls=%async_computation.5 | async-start | bytes 2097152 | tf_op jit(solution)/shard_map/psum | solution.py:80
  8.7 47.7 %slice-start = ((s8[8388608]{0:T(1024)(128)(4,1)}), s8[4194304]{0:T(1024)(128)(4,1)S(1)}, s32[]{:S(2)}) async-start(s8[8388608]{0:T(1024)(128)(4,1)} %bitcast.30), calls=%async_computation.6 | async-start | bytes 8388608
  42.4 14.0 %slice-start.1 = ((s8[8388608]{0:T(1024)(128)(4,1)}), s8[4194304]{0:T(1024)(128)(4,1)S(1)}, s32[]{:S(2)}) async-start(s8[8388608]{0:T(1024)(128)(4,1)} %bitcast.30), calls=%async_computation.7 | async-start | bytes 8388608
  49.0 7.5 %copy-start.15 = (bf16[1024,512]{1,0:T(8,128)(2,1)S(1)}, bf16[1024,512]{1,0:T(8,128)(2,1)}, u32[]{:S(2)}) copy-start(bf16[1024,512]{1,0:T(8,128)(2,1)} %param.19) | copy-start | bytes 3145732
  56.4 6.8 %copy-start.16 = (bf16[1024,512]{1,0:T(8,128)(2,1)S(1)}, bf16[1024,512]{1,0:T(8,128)(2,1)}, u32[]{:S(2)}) copy-start(bf16[1024,512]{1,0:T(8,128)(2,1)} %param.20) | copy-start | bytes 3145732
  70.0 36.3 %copy-start.11 = (f32[128,512]{1,0:T(8,128)S(1)}, f32[128,512]{1,0:T(8,128)}, u32[]{:S(2)}) copy-start(f32[128,512]{1,0:T(8,128)} %param.28) | copy-start | bytes 786436
  70.0 36.5 %copy-start.12 = (f32[128,512]{1,0:T(8,128)S(1)}, f32[128,512]{1,0:T(8,128)}, u32[]{:S(2)}) copy-start(f32[128,512]{1,0:T(8,128)} %param.29) | copy-start | bytes 786436
  70.0 36.6 %copy-start.13 = (f32[128,512]{1,0:T(8,128)S(1)}, f32[128,512]{1,0:T(8,128)}, u32[]{:S(2)}) copy-start(f32[128,512]{1,0:T(8,128)} %param.31) | copy-start | bytes 786436
  81.1 25.6 %copy-start.14 = (f32[128,512]{1,0:T(8,128)S(1)}, f32[128,512]{1,0:T(8,128)}, u32[]{:S(2)}) copy-start(f32[128,512]{1,0:T(8,128)} %param.32) | copy-start | bytes 786436
  81.1 25.8 %copy-start.8 = (f32[128,1024]{1,0:T(8,128)S(1)}, f32[128,1024]{1,0:T(8,128)}, u32[]{:S(2)}) copy-start(f32[128,1024]{1,0:T(8,128)} %param.30) | copy-start | bytes 1572868
  81.1 26.0 %copy-start.9 = (f32[128,1024]{1,0:T(8,128)S(1)}, f32[128,1024]{1,0:T(8,128)}, u32[]{:S(2)}) copy-start(f32[128,1024]{1,0:T(8,128)} %param.33) | copy-start | bytes 1572868
  81.1 103.7 %copy-start.10 = (bf16[256,128]{1,0:T(8,128)(2,1)S(1)}, bf16[256,128]{1,0:T(8,128)(2,1)}, u32[]{:S(2)}) copy-start(bf16[256,128]{1,0:T(8,128)(2,1)} %param.27) | copy-start | bytes 196612
  106.2 81.0 %copy-start.7 = (bf16[512,128]{1,0:T(8,128)(2,1)S(1)}, bf16[512,128]{1,0:T(8,128)(2,1)}, u32[]{:S(2)}) copy-start(bf16[512,128]{1,0:T(8,128)(2,1)} %param.26) | copy-start | bytes 393220
  106.3 207.3 %all-gather.12.cloned.1.call-start = ((), (), s32[]{:S(2)}) async-start(), calls=%async_computation.3 | async-start | bytes 4718592 | tf_op jit(solution)/shard_map/all_gather | solution.py:101
  187.2 2.2 copy-start.4
  187.2 4.4 copy-start.6
  239.6 148.8 %all-gather.14.cloned.1.call-start = ((), (), s32[]{:S(2)}) async-start(), calls=%async_computation.4 | async-start | bytes 4718592 | tf_op jit(solution)/shard_map/all_gather | solution.py:104
  244.7 13.7 %copy-start.2 = (f32[512,512]{0,1:T(8,128)S(1)}, f32[512,512]{0,1:T(8,128)}, u32[]{:S(2)}) copy-start(f32[512,512]{0,1:T(8,128)} %get-tuple-element.30) | copy-start | bytes 3145732
  244.7 218.9 %all-gather.10.cloned.1.call-start = ((), (), s32[]{:S(2)}) async-start(), calls=%async_computation.2 | async-start | bytes 4718592 | tf_op jit(solution)/shard_map/all_gather | solution.py:98
  250.1 12.1 %copy-start.3 = (f32[512,512]{0,1:T(8,128)S(1)}, f32[512,512]{0,1:T(8,128)}, u32[]{:S(2)}) copy-start(f32[512,512]{0,1:T(8,128)} %get-tuple-element.32) | copy-start | bytes 3145732
  313.6 156.5 %copy-start.1 = (bf16[1024,1024]{1,0:T(8,128)(2,1)S(1)}, bf16[1024,1024]{1,0:T(8,128)(2,1)}, u32[]{:S(2)}) copy-start(bf16[1024,1024]{1,0:T(8,128)(2,1)} %param.21) | copy-start | bytes 6291460
  (1 other events, 2.2 us)
Sparse Core Ops, SparseCore 0:
  10.1 43.7 all-gather.5
  56.0 38.9 all-gather.7
  106.4 77.2 all-reduce.2
  239.7 73.8 all-gather.11
  315.5 72.8 all-gather.13
  390.8 72.8 all-gather.9
where the time goes:
time: 478 us; the launch traced here: 477 us
  waiting for transfers between devices  279 us (58%)
  blocking collectives  73.4 us (15%)
  matrix products  55.4 us (12%)
  local copies, waits for them, and re-layouts  41.4 us (9%)
  between operations  17 us (4%)
  other arithmetic  10.5 us (2%)
    psum x1, waiting for transfers between devices, local(): lax.psum((first_sum, second_sum, part_output), 'fs')  76.3 us
    all_gather x1, waiting for transfers between devices, local(): lax.all_gather((query_weight + learn_rate * query_step).astype(jnp.bfloat...  68.9 us
    all_gather x1, waiting for transfers between devices, local(): lax.all_gather((output_weight + learn_rate * output_step).astype(jnp.bflo...  68.2 us
    all_gather x1, waiting for transfers between devices, local(): lax.all_gather((value_weight + learn_rate * value_step).astype(jnp.bfloat...  50 us
    unnamed x59, local copies, waits for them, and re-layouts  41.4 us
    psum x1, blocking collectives, local(): squares = lax.psum(partial_squares, ('fs', 'tp'))  39.8 us
    all_gather x1, blocking collectives, local(): lax.all_gather(output_basis, 'fs', axis=0, tiled=True).astype(jnp.float32)  33.7 us
    dot_general x3, matrix products, across_exact(): lax.dot_general(leading, trailing, (((0,), (0,)), ((), ())), precision=la...  29.7 us
  transfers between devices with their start and end apart: 6, of which 5 were waited for; matrix products, arithmetic and copies ran while one was open for 16% of the time, Pallas kernels for 0%

commit v1 on v0

v1 whole, which is shorter than its diff:
```python
import jax
import jax.numpy as jnp
from jax import lax
from jax.experimental import pallas as pl
from jax.experimental.pallas import tpu as pltpu
from jax.sharding import PartitionSpec as P

beta_first = 0.8
beta_second = 0.9
floor_mean = 0.005
learn_rate = 0.05

STREAMS = 2
BF = jnp.bfloat16
F32 = jnp.float32
ANY = pl.BlockSpec(memory_space=pl.ANY)
SMEM = pl.BlockSpec(memory_space=pltpu.SMEM)
VM = pl.BlockSpec(memory_space=pltpu.VMEM)
LIMIT = 48 * 1024 * 1024


def pack(q, v, o, pieces):
    rq, cq = q.shape
    ro, co = o.shape
    a, b, r = rq // pieces, ro // pieces, co // cq

    def body(q_ref, v_ref, o_ref, *outs):
        for p in range(pieces):
            outs[p][0:a, :] = q_ref[p * a : (p + 1) * a, :].astype(BF)
            outs[p][a : 2 * a, :] = v_ref[p * a : (p + 1) * a, :].astype(BF)
            for c in range(r):
                outs[p][2 * a + c * b : 2 * a + (c + 1) * b, :] = o_ref[
                    p * b : (p + 1) * b, c * cq : (c + 1) * cq
                ].astype(BF)

    shape = jax.ShapeDtypeStruct((2 * a + r * b, cq), BF)
    return pl.pallas_call(
        body,
        out_shape=(shape,) * pieces,
        in_specs=[VM] * 3,
        out_specs=(VM,) * pieces,
        compiler_params=pltpu.CompilerParams(vmem_limit_bytes=LIMIT),
        name="pack",
    )(q, v, o)


def project(index, x, y, gq, gv, go, parts, n, m, rq, ro, rank):
    tokens = x.shape[0]
    steps = 4
    tt = tokens // steps
    cq, co = gq.shape[1], go.shape[1]
    cols = 2 * cq + co
    seg = rank // n
    aq, ao = rq // m, ro // m

    def body(index_ref, x_ref, y_ref, gq_ref, gv_ref, go_ref, *rest):
        part_refs = rest[:m]
        own_ref = rest[m]
        seg_refs = rest[m + 1 : m + n]
        bqv_ref, bo_ref, gram_ref = rest[m + n : m + n + 3]
        xs, ys, proj, sem_b, sem_o, sem_x, sem_y = rest[m + n + 3 :]
        for e in range(m):
            lane = index_ref[n + e]
            for d in range(n):
                row = index_ref[d]
                rows = pl.ds(pl.multiple_of(row * rq + lane * aq, aq), aq)
                pltpu.make_async_copy(
                    part_refs[e].at[d, pl.ds(0, aq), :], bqv_ref.at[rows, pl.ds(0, rank)], sem_b
                ).start()
                pltpu.make_async_copy(
                    part_refs[e].at[d, pl.ds(aq, aq), :], bqv_ref.at[rows, pl.ds(rank, rank)], sem_b
                ).start()
                rows = pl.ds(pl.multiple_of(row * ro + lane * ao, ao), ao)
                pltpu.make_async_copy(
                    part_refs[e].at[d, pl.ds(2 * aq, ao), :], bo_ref.at[rows, :], sem_o
                ).start()

        def copies(s):
            rows = pl.ds(s * tt, tt)
            return (
                pltpu.make_async_copy(x_ref.at[rows, :], xs.at[s], sem_x.at[s]),
                pltpu.make_async_copy(y_ref.at[rows, :], ys.at[s], sem_y.at[s]),
            )

        for s in range(steps):
            for copy in copies(s):
                copy.start()
        pltpu.make_async_copy(bqv_ref, bqv_ref, sem_b).wait()
        pltpu.make_async_copy(bo_ref, bo_ref, sem_o).wait()
        for s in range(steps):
            for copy in copies(s):
                copy.wait()
            rows = slice(s * tt, (s + 1) * tt)
            xb = jnp.dot(xs[s], bqv_ref[...], preferred_element_type=F32).T
            yb = jnp.dot(ys[s], bo_ref[...], preferred_element_type=F32).T
            for left, grad, lo, hi in (
                (xb[0:rank], gq_ref, 0, cq),
                (xb[rank : 2 * rank], gv_ref, cq, 2 * cq),
                (yb, go_ref, 2 * cq, cols),
            ):
                top = left.astype(BF)
                low = (left - top.astype(F32)).astype(BF)
                right = grad[rows, :]
                value = jnp.dot(top, right, preferred_element_type=F32) + jnp.dot(
                    low, right, preferred_element_type=F32
                )
                if s == 0:
                    proj[:, lo:hi] = value
                else:
                    proj[:, lo:hi] = proj[:, lo:hi] + value
        own_ref[...] = proj[pl.ds(pl.multiple_of(index_ref[0] * seg, seg), seg), :]
        for d in range(1, n):
            seg_refs[d - 1][...] = proj[
                pl.ds(pl.multiple_of(index_ref[d] * seg, seg), seg), :
            ].astype(BF)
        inner = (((0,), (0,)), ((), ()))
        both = lax.dot_general(bqv_ref[...], bqv_ref[...], inner, preferred_element_type=F32)
        gram_ref[0] = both[0:rank, 0:rank]
        gram_ref[1] = both[rank:, rank:]
        gram_ref[2] = lax.dot_general(bo_ref[...], bo_ref[...], inner, preferred_element_type=F32)

    outs = (
        [jax.ShapeDtypeStruct((seg, cols), F32)]
        + [jax.ShapeDtypeStruct((seg, cols), BF)] * (n - 1)
        + [
            jax.ShapeDtypeStruct((n * rq, 2 * rank), BF),
            jax.ShapeDtypeStruct((n * ro, rank), BF),
            jax.ShapeDtypeStruct((3, rank, rank), F32),
        ]
    )
    return pl.pallas_call(
        body,
        out_shape=tuple(outs),
        in_specs=[SMEM, ANY, ANY, VM, VM, VM] + [ANY] * m,
        out_specs=tuple([VM] * len(outs)),
        scratch_shapes=[
            pltpu.VMEM((steps, tt, x.shape[1]), BF),
            pltpu.VMEM((steps, tt, y.shape[1]), BF),
            pltpu.VMEM((rank, cols), F32),
            pltpu.SemaphoreType.DMA,
            pltpu.SemaphoreType.DMA,
            pltpu.SemaphoreType.DMA((steps,)),
            pltpu.SemaphoreType.DMA((steps,)),
        ],
        compiler_params=pltpu.CompilerParams(vmem_limit_bytes=LIMIT),
        name="project",
    )(index, x, y, gq, gv, go, *parts)


def halves(value):
    top = value.astype(BF)
    return top, (value - top.astype(F32)).astype(BF)


def moments(index, segs, means, squares, gram, n, rank):
    widths = [w.shape[1] for w in means]
    cols = sum(widths)
    seg = rank // n

    def body(index_ref, *rest):
        seg_refs = rest[:n]
        mean_refs = rest[n : n + 3]
        square_refs = rest[n + 3 : n + 6]
        gram_ref = rest[n + 6]
        first_refs = rest[n + 7 : n + 10]
        second_refs = rest[n + 10 : n + 13]
        top_ref, low_ref, sum_ref, proj = rest[n + 13 :]
        for d in range(n):
            proj[pl.ds(pl.multiple_of(index_ref[d] * seg, seg), seg), :] = seg_refs[d][...].astype(F32)
        at = 0
        total = jnp.zeros((1, 1), F32)
        for k in range(3):
            w = widths[k]
            value = proj[:, at : at + w]
            first = beta_first * mean_refs[k][...] + (1.0 - beta_first) * value
            second = beta_second * square_refs[k][...] + (1.0 - beta_second) * value * value
            first_refs[k][...] = first
            second_refs[k][...] = second
            direction = first / jnp.sqrt(second)
            top, low = halves(direction)
            top_ref[:, at : at + w] = top
            low_ref[:, at : at + w] = low
            g_top, g_low = halves(gram_ref[k])
            applied = (
                jnp.dot(g_top, top, preferred_element_type=F32)
                + jnp.dot(g_top, low, preferred_element_type=F32)
                + jnp.dot(g_low, top, preferred_element_type=F32)
            )
            total = total + jnp.sum(direction * applied, keepdims=True)
            at += w
        sum_ref[...] = jnp.broadcast_to(total, sum_ref.shape)

    outs = [jax.ShapeDtypeStruct((rank, w), F32) for w in widths] * 2 + [
        jax.ShapeDtypeStruct((rank, cols), BF),
        jax.ShapeDtypeStruct((rank, cols), BF),
        jax.ShapeDtypeStruct((8, 128), F32),
    ]
    return pl.pallas_call(
        body,
        out_shape=tuple(outs),
        in_specs=[SMEM] + [VM] * (n + 7),
        out_specs=tuple([VM] * len(outs)),
        scratch_shapes=[pltpu.VMEM((rank, cols), F32)],
        compiler_params=pltpu.CompilerParams(vmem_limit_bytes=LIMIT),
        name="moments",
    )(index, *segs, *means, *squares, gram)


def factor_of(sum_refs, count):
    values = [ref[0:1, 0:1] for ref in sum_refs]
    while len(values) > 1:
        values = [values[i] + values[i + 1] for i in range(0, len(values), 2)]
    return 1.0 / jnp.sqrt(values[0] / count + floor_mean)


def steps_of(rows, top, low, bqv, bo, sums, count, rq, ro, cq, co, rank):
    def body(index_ref, top_ref, low_ref, bqv_ref, bo_ref, *rest):
        sum_refs = rest[: len(sums)]
        q_ref, v_ref, o_ref = rest[len(sums) :]
        scale = -factor_of(sum_refs, count)

        def lowrank(basis, lo, hi):
            return jnp.dot(basis, top_ref[:, lo:hi], preferred_element_type=F32) + jnp.dot(
                basis, low_ref[:, lo:hi], preferred_element_type=F32
            )

        mine = pl.ds(pl.multiple_of(index_ref[0] * rq, rq), rq)
        q_ref[...] = scale * lowrank(bqv_ref[mine, 0:rank], 0, cq)
        v_ref[...] = scale * lowrank(bqv_ref[mine, rank : 2 * rank], cq, 2 * cq)
        mine = pl.ds(pl.multiple_of(index_ref[0] * ro, ro), ro)
        o_ref[...] = scale * lowrank(bo_ref[mine, :], 2 * cq, 2 * cq + co)

    outs = [jax.ShapeDtypeStruct((rq, cq), F32)] * 2 + [jax.ShapeDtypeStruct((ro, co), F32)]
    return pl.pallas_call(
        body,
        out_shape=tuple(outs),
        in_specs=[SMEM] + [VM] * (4 + len(sums)),
        out_specs=tuple([VM] * 3),
        compiler_params=pltpu.CompilerParams(vmem_limit_bytes=LIMIT),
        name="steps",
    )(rows, top, low, bqv, bo, *sums)


def write_copies(rows, labels, pieces, top, bqv, bo, sums, count, old, n, total, rq, ro, cq, co, rank):
    a, b, r = rq // total, ro // total, co // cq
    k = len(pieces)
    s = len(sums)

    def body(index_ref, top_ref, bqv_ref, bo_ref, *rest):
        sum_refs = rest[:s]
        piece_refs = rest[s : s + k]
        rest = rest[s + k + (3 if old else 0) :]
        q_out, v_out, o_out, q_buf, v_buf, o_buf, sem = rest
        scale = -learn_rate * factor_of(sum_refs, count)
        copies = []
        for i in range(k):
            piece = piece_refs[i]
            at = index_ref[i]
            here = pl.ds(pl.multiple_of(at * rq + labels[i] * a, a), a)
            there = pl.ds(pl.multiple_of(at * ro + labels[i] * b, b), b)
            low = jnp.dot(bqv_ref[here, 0:rank], top_ref[:, 0:cq], preferred_element_type=F32)
            q_buf[i] = (piece[0:a, :].astype(F32) + scale * low).astype(BF)
            copies.append(pltpu.make_async_copy(q_buf.at[i], q_out.at[here, :], sem.at[3 * i]))
            copies[-1].start()
            low = jnp.dot(
                bqv_ref[here, rank : 2 * rank], top_ref[:, cq : 2 * cq], preferred_element_type=F32
            )
            v_buf[i] = (piece[a : 2 * a, :].astype(F32) + scale * low).astype(BF)
            copies.append(pltpu.make_async_copy(v_buf.at[i], v_out.at[here, :], sem.at[3 * i + 1]))
            copies[-1].start()
            low = jnp.dot(bo_ref[there, :], top_ref[:, 2 * cq :], preferred_element_type=F32)
            for c in range(r):
                old_rows = piece[2 * a + c * b : 2 * a + (c + 1) * b, :].astype(F32)
                o_buf[i, :, c * cq : (c + 1) * cq] = (
                    old_rows + scale * low[:, c * cq : (c + 1) * cq]
                ).astype(BF)
            copies.append(pltpu.make_async_copy(o_buf.at[i], o_out.at[there, :], sem.at[3 * i + 2]))
            copies[-1].start()
        for copy in copies:
            copy.wait()

    outs = (
        jax.ShapeDtypeStruct((n * rq, cq), BF),
        jax.ShapeDtypeStruct((n * rq, cq), BF),
        jax.ShapeDtypeStruct((n * ro, co), BF),
    )
    before = 4 + s + k
    return pl.pallas_call(
        body,
        out_shape=outs,
        in_specs=[SMEM] + [VM] * (3 + s + k) + ([ANY] * 3 if old else []),
        out_specs=(ANY,) * 3,
        input_output_aliases={before + i: i for i in range(3)} if old else {},
        scratch_shapes=[
            pltpu.VMEM((k, a, cq), BF),
            pltpu.VMEM((k, a, cq), BF),
            pltpu.VMEM((k, b, co), BF),
            pltpu.SemaphoreType.DMA((3 * k,)),
        ],
        compiler_params=pltpu.CompilerParams(vmem_limit_bytes=LIMIT),
        name="copies",
    )(rows, top, bqv, bo, *sums, *pieces, *(old or ()))


def solution(mesh):
    n = mesh.shape["fs"]
    m = mesh.shape["tp"]
    order = list(range(0, n, 2)) + list(range(n - 1 - n % 2, 0, -2))
    place = [order.index(i) for i in range(n)]
    onward = [(order[i], order[(i + 1) % n]) for i in range(n)]
    back = [(d, s) for s, d in onward]

    def swap(x, axis, bits):
        size = mesh.shape[axis]
        return lax.ppermute(x, axis, [(i, i ^ bits) for i in range(size)])

    def local(x, y, gq, gv, go, wq, wv, wo, bq, bv, bo, mq, mv, mo, sq, sv, so):
        rq, cq = wq.shape
        ro, co = wo.shape
        rank = bq.shape[1]
        count = float(2 * n * rq * m * cq + n * ro * m * co)
        me = lax.axis_index("fs")
        lane = lax.axis_index("tp")
        pieces = 2 * STREAMS

        packed = pack(wq, wv, wo, pieces)

        aq, ao = rq // m, ro // m
        share = jnp.concatenate(
            [
                lax.dynamic_slice_in_dim(bq, lane * aq, aq, 0),
                lax.dynamic_slice_in_dim(bv, lane * aq, aq, 0),
                lax.dynamic_slice_in_dim(bo, lane * ao, ao, 0),
            ]
        )
        parts = [jnp.stack([share] + [swap(share, "fs", d) for d in range(1, n)])]
        offsets = [0]
        bit = m // 2
        while bit:
            parts = parts + [swap(part, "tp", bit) for part in parts]
            offsets = offsets + [e ^ bit for e in offsets]
            bit //= 2
        index = jnp.stack([me ^ d for d in range(n)] + [lane ^ e for e in offsets]).astype(jnp.int32)

        arrived = [[] for _ in range(n)]
        walk = jnp.asarray(order, jnp.int32)
        spot = jnp.asarray(place, jnp.int32)[me]
        arrived[0] = [(packed[p], p, me) for p in range(pieces)]
        for p in range(pieces):
            piece = packed[p]
            for k in range(1, n):
                piece = lax.ppermute(piece, "fs", back if p % 2 else onward)
                source = walk[(spot + k) % n] if p % 2 else walk[(spot - k) % n]
                arrived[k].append((piece, p, source))

        out = project(index, x, y, gq, gv, go, parts, n, m, rq, ro, rank)
        own, given, (bqv, bo_all, gram) = out[0], out[1:n], out[n:]
        total = own
        for d in range(1, n):
            total = total + swap(given[d - 1], "fs", d).astype(F32)
        total = total.astype(BF)
        segs = [total] + [swap(total, "fs", d) for d in range(1, n)]
        out = moments(index, segs, (mq, mv, mo), (sq, sv, so), gram, n, rank)
        firsts, seconds, (top, low, part_sum) = out[0:3], out[3:6], out[6:]
        sums = [part_sum] + [swap(part_sum, "tp", e) for e in range(1, m)]
        steps = steps_of(index, top, low, bqv, bo_all, sums, count, rq, ro, cq, co, rank)
        old = None
        cut = max(n - 3, 1)
        for group in [range(0, cut)] + [[k] for k in range(cut, n)]:
            some = [item for k in group for item in arrived[k]]
            rows = jnp.stack([item[2] for item in some]).astype(jnp.int32)
            old = write_copies(
                rows,
                [item[1] for item in some],
                [item[0] for item in some],
                top,
                bqv,
                bo_all,
                sums,
                count,
                old,
                n,
                pieces,
                rq,
                ro,
                cq,
                co,
                rank,
            )
        return (*steps, *old, *firsts, *seconds)

    rows = P("fs", None)
    both = P("fs", "tp")
    cols = P(None, "tp")
    return jax.shard_map(
        local,
        mesh=mesh,
        in_specs=(rows, rows) + (both,) * 6 + (rows,) * 3 + (cols,) * 6,
        out_specs=(both,) * 3 + (cols,) * 9,
        check_vma=False,
    )
```

time: 478 us -> 266 us (0.56)
  waiting for transfers between devices: 279 us -> 99.9 us
  blocking collectives: 73.4 us -> 0 us
  starting transfers between devices: 0.24 us -> 64.4 us
  matrix products: 55.4 us -> 0 us
  Pallas kernels: 0 us -> 35.5 us
  local copies, waits for them, and re-layouts: 41.4 us -> 49.8 us
  other arithmetic: 10.5 us -> 4.16 us
  between operations: 17 us -> 10.7 us
    all_gather x5 -> x0, waiting for transfers between devices: 201 us -> none  [the longest x1 68.9 us: local(): lax.all_gather((query_weight + learn_rate * query_step).astype(jnp.bfloat...]
    ppermute x0 -> x55, waiting for transfers between devices: none -> 99.9 us  [the longest x27 65.9 us: swap(): return lax.ppermute(x, axis, [(i, i ^ bits) for i in range(size)])]
    psum x1 -> x0, waiting for transfers between devices: 76.3 us -> none  [local(): lax.psum((first_sum, second_sum, part_output), 'fs')]
    ppermute x0 -> x55, starting transfers between devices: none -> 64.4 us  [the longest x27 39.4 us: swap(): return lax.ppermute(x, axis, [(i, i ^ bits) for i in range(size)])]
    dot_general x9 -> x0, matrix products: 55.4 us -> none  [the longest x3 29.7 us: across_exact(): lax.dot_general(leading, trailing, (((0,), (0,)), ((), ())), precision=la...]
    psum x1 -> x0, blocking collectives: 39.8 us -> none  [local(): squares = lax.psum(partial_squares, ('fs', 'tp'))]
    pallas_call x0 -> x8, Pallas kernels: none -> 35.5 us  [the longest x1 15.2 us: project(): pl.pallas_call(body, out_shape=tuple(outs), in_specs=[SMEM, ANY, ANY, VM,...]
    all_gather x1 -> x0, blocking collectives: 33.7 us -> none  [local(): lax.all_gather(output_basis, 'fs', axis=0, tiled=True).astype(jnp.float32)]
  transfers between devices with their start and end apart: 6 -> 55, of which waited for: 5 -> 21; matrix products, arithmetic and copies ran while one was open for 16% -> 6% of each run, Pallas kernels for 0% -> 12%
where the time goes in v1:
time: 266 us; the launch traced here: 264 us
  waiting for transfers between devices  99.9 us (38%)
  starting transfers between devices  64.4 us (24%)
  local copies, waits for them, and re-layouts  49.8 us (19%)
  Pallas kernels  35.5 us (13%)
  between operations  10.7 us (4%)
  other arithmetic  4.16 us (2%)
    ppermute x27, waiting for transfers between devices, swap(): return lax.ppermute(x, axis, [(i, i ^ bits) for i in range(size)])  65.9 us
    ppermute x27, starting transfers between devices, swap(): return lax.ppermute(x, axis, [(i, i ^ bits) for i in range(size)])  39.4 us
    unnamed x138, local copies, waits for them, and re-layouts  37.7 us
    ppermute x28, waiting for transfers between devices, local(): piece = lax.ppermute(piece, 'fs', back if p % 2 else onward)  34 us
    ppermute x28, starting transfers between devices, local(): piece = lax.ppermute(piece, 'fs', back if p % 2 else onward)  24.9 us
    pallas_call x1, Pallas kernels, project(): pl.pallas_call(body, out_shape=tuple(outs), in_specs=[SMEM, ANY, ANY, VM,...  15.2 us
    pallas_call x4, Pallas kernels, write_copies(): pl.pallas_call(body, out_shape=outs, in_specs=[SMEM] + [VM] * (3 + s + k)...  14.8 us
    another operation x1, local copies, waits for them, and re-layouts, local(): rows = jnp.stack([item[2] for item in some]).astype(jnp.int32)  9.91 us
  transfers between devices with their start and end apart: 55, of which 21 were waited for; matrix products, arithmetic and copies ran while one was open for 6% of the time, Pallas kernels for 12%

profile of v1, /device:TPU:0, one launch (start us, length us, event | category | flops | bytes accessed | tf_op | source)
XLA Modules:
  0.0 264.4 jit_solution(17877303327372672948)
XLA Ops:
  2.3 3.0 %collective-permute-start = (bf16[320,128]{1,0:T(8,128)(2,1)S(1)}, bf16[320,128]{1,0:T(8,128)(2,1)S(1)}, u32[]{:S(2)}, u32[]{:S(2)}) collective-permute-start(bf16[320,128]{1,0:T(8,128)(2,1)S(1)} %pad_maximum_fusion), channel_id=1, source_target_pairs={{0,4},{4,0},{8,12},{12,8},{16,20},{20,16},{24,28},{28,24},{1,5},{5... | collective-permute-start | bytes 245768 | tf_op jit(solution)/shard_map/ppermute | solution.py:315
  15.1 3.7 %collective-permute-start.5 = (bf16[320,128]{1,0:T(8,128)(2,1)S(1)}, bf16[320,128]{1,0:T(8,128)(2,1)S(1)}, u32[]{:S(2)}, u32[]{:S(2)}) collective-permute-start(bf16[320,128]{1,0:T(8,128)(2,1)S(1)} %pad_maximum_fusion), channel_id=1, source_target_pairs={{0,24},{4,28},{8,16},{12,20},{16,8},{20,12},{24,0},{28,4},{1,25},{... | collective-permute-start | bytes 245768 | tf_op jit(solution)/shard_map/ppermute | solution.py:315
  21.6 5.3 %collective-permute-done.6 = bf16[320,128]{1,0:T(8,128)(2,1)S(1)} collective-permute-done((bf16[320,128]{1,0:T(8,128)(2,1)S(1)}, bf16[320,128]{1,0:T(8,128)(2,1)S(1)}, u32[]{:S(2)}, u32[]{:S(2)}) %collective-permute-start.6) | collective-permute-done | bytes 81952 | tf_op jit(solution)/shard_map/ppermute | solution.py:315
  32.8 7.6 %collective-permute-done.34.rest_9_ = bf16[384,512]{1,0:T(8,128)(2,1)S(1)} collective-permute-done((bf16[384,512]{1,0:T(8,128)(2,1)S(1)}, bf16[384,512]{1,0:T(8,128)(2,1)S(1)}, u32[]{:S(2)}, u32[]{:S(2)}) %collective-permute-start.34) | collective-permute-done | bytes 393248 | tf_op jit(solution)/shard_map/ppermute | solution.py:352
  44.0 4.9 %collective-permute-done.48.rest_11_ = bf16[384,512]{1,0:T(8,128)(2,1)S(1)} collective-permute-done((bf16[384,512]{1,0:T(8,128)(2,1)S(1)}, bf16[384,512]{1,0:T(8,128)(2,1)S(1)}, u32[]{:S(2)}, u32[]{:S(2)}) %collective-permute-start.48) | collective-permute-done | bytes 393248 | tf_op jit(solution)/shard_map/ppermute | solution.py:352
  53.5 3.9 %collective-permute-done.35.rest_13_ = bf16[384,512]{1,0:T(8,128)(2,1)} collective-permute-done((bf16[384,512]{1,0:T(8,128)(2,1)S(1)}, bf16[384,512]{1,0:T(8,128)(2,1)}, u32[]{:S(2)}, u32[]{:S(2)}) %collective-permute-start.35) | collective-permute-done | bytes 393248 | tf_op jit(solution)/shard_map/ppermute | solution.py:352
  57.4 3.6 %collective-permute-done.42.rest_14_ = bf16[384,512]{1,0:T(8,128)(2,1)} collective-permute-done((bf16[384,512]{1,0:T(8,128)(2,1)S(1)}, bf16[384,512]{1,0:T(8,128)(2,1)}, u32[]{:S(2)}, u32[]{:S(2)}) %collective-permute-start.42) | collective-permute-done | bytes 393248 | tf_op jit(solution)/shard_map/ppermute | solution.py:352
  61.1 4.7 %collective-permute-done.49.rest_15_ = bf16[384,512]{1,0:T(8,128)(2,1)} collective-permute-done((bf16[384,512]{1,0:T(8,128)(2,1)S(1)}, bf16[384,512]{1,0:T(8,128)(2,1)}, u32[]{:S(2)}, u32[]{:S(2)}) %collective-permute-start.49) | collective-permute-done | bytes 393248 | tf_op jit(solution)/shard_map/ppermute | solution.py:352
  67.0 15.2 %project.1 = (f32[16,2048]{1,0:T(8,128)S(1)}, bf16[16,2048]{1,0:T(8,128)(2,1)S(1)}, bf16[16,2048]{1,0:T(8,128)(2,1)S(1)}, bf16[16,2048]{1,0:T(8,128)(2,1)S(1)}, ...) custom-call(s32[12]{0:T(128)S(1)} %stack.94.index_ref, ...), custom_call_target="tpu_custom_call" | custom-call | tf_op jit(solution)/shard_map/project/pallas_call | solution.py:131
  90.8 15.1 %collective-permute-done.12 = bf16[16,2048]{1,0:T(8,128)(2,1)S(1)} collective-permute-done((bf16[16,2048]{1,0:T(8,128)(2,1)S(1)}, bf16[16,2048]{1,0:T(8,128)(2,1)S(1)}, u32[]{:S(2)}, u32[]{:S(2)}) %collective-permute-start.12) | collective-permute-done | bytes 65568 | tf_op jit(solution)/shard_map/ppermute | solution.py:315
  106.5 4.6 %collective-permute-done.13 = bf16[16,2048]{1,0:T(8,128)(2,1)S(1)} collective-permute-done((bf16[16,2048]{1,0:T(8,128)(2,1)S(1)}, bf16[16,2048]{1,0:T(8,128)(2,1)S(1)}, u32[]{:S(2)}, u32[]{:S(2)}) %collective-permute-start.13) | collective-permute-done | bytes 65568 | tf_op jit(solution)/shard_map/ppermute | solution.py:315
  113.5 4.2 %collective-permute-done.14 = bf16[16,2048]{1,0:T(8,128)(2,1)S(1)} collective-permute-done((bf16[16,2048]{1,0:T(8,128)(2,1)S(1)}, bf16[16,2048]{1,0:T(8,128)(2,1)S(1)}, u32[]{:S(2)}, u32[]{:S(2)}) %collective-permute-start.14) | collective-permute-done | bytes 65568 | tf_op jit(solution)/shard_map/ppermute | solution.py:315
  117.7 3.1 %collective-permute-start.15 = (bf16[16,2048]{1,0:T(8,128)(2,1)S(1)}, bf16[16,2048]{1,0:T(8,128)(2,1)S(1)}, u32[]{:S(2)}, u32[]{:S(2)}) collective-permute-start(bf16[16,2048]{1,0:T(8,128)(2,1)S(1)} %get-tuple-element.57), channel_id=1, source_target_pairs={{0,24},{4,28},{8,16},{12,20},{16,8},{20,12},{24,0},{28,4},{1,25},{... | collective-permute-start | bytes 196616 | tf_op jit(solution)/shard_map/ppermute | solution.py:315
  120.8 3.1 %collective-permute-done.15 = bf16[16,2048]{1,0:T(8,128)(2,1)S(1)} collective-permute-done((bf16[16,2048]{1,0:T(8,128)(2,1)S(1)}, bf16[16,2048]{1,0:T(8,128)(2,1)S(1)}, u32[]{:S(2)}, u32[]{:S(2)}) %collective-permute-start.15) | collective-permute-done | bytes 65568 | tf_op jit(solution)/shard_map/ppermute | solution.py:315
  131.6 3.5 %collective-permute-start.17 = (bf16[16,2048]{1,0:T(8,128)(2,1)S(1)}, bf16[16,2048]{1,0:T(8,128)(2,1)S(1)}, u32[]{:S(2)}, u32[]{:S(2)}) collective-permute-start(bf16[16,2048]{1,0:T(8,128)(2,1)S(1)} %add_convert_fusion.rest_0_), channel_id=1, source_target_pairs={{0,4},{4,0},{8,12},{12,8},{16,20},{20,16},{24,28},{28,24},{1,5},{5... | collective-permute-start | bytes 196616 | tf_op jit(solution)/shard_map/ppermute | solution.py:315
  135.1 4.4 %collective-permute-done.31.rest_4_ = bf16[384,512]{1,0:T(8,128)(2,1)S(1)} collective-permute-done((bf16[384,512]{1,0:T(8,128)(2,1)S(1)}, bf16[384,512]{1,0:T(8,128)(2,1)S(1)}, u32[]{:S(2)}, u32[]{:S(2)}) %collective-permute-start.31) | collective-permute-done | bytes 393248 | tf_op jit(solution)/shard_map/ppermute | solution.py:352
  143.1 4.9 %collective-permute-done.45.rest_6_ = bf16[384,512]{1,0:T(8,128)(2,1)S(1)} collective-permute-done((bf16[384,512]{1,0:T(8,128)(2,1)S(1)}, bf16[384,512]{1,0:T(8,128)(2,1)S(1)}, u32[]{:S(2)}, u32[]{:S(2)}) %collective-permute-start.45) | collective-permute-done | bytes 393248 | tf_op jit(solution)/shard_map/ppermute | solution.py:352
  151.9 8.4 %collective-permute-done.18.rest_2_ = bf16[16,2048]{1,0:T(8,128)(2,1)S(1)} collective-permute-done((bf16[16,2048]{1,0:T(8,128)(2,1)S(1)}, bf16[16,2048]{1,0:T(8,128)(2,1)S(1)}, u32[]{:S(2)}, u32[]{:S(2)}) %collective-permute-start.18) | collective-permute-done | bytes 65568 | tf_op jit(solution)/shard_map/ppermute | solution.py:315
  161.9 3.5 %collective-permute-done.19.rest_3_ = bf16[16,2048]{1,0:T(8,128)(2,1)S(1)} collective-permute-done((bf16[16,2048]{1,0:T(8,128)(2,1)S(1)}, bf16[16,2048]{1,0:T(8,128)(2,1)S(1)}, u32[]{:S(2)}, u32[]{:S(2)}) %collective-permute-start.19) | collective-permute-done | bytes 65568 | tf_op jit(solution)/shard_map/ppermute | solution.py:315
  165.4 3.9 %collective-permute-start.20 = (bf16[16,2048]{1,0:T(8,128)(2,1)S(1)}, bf16[16,2048]{1,0:T(8,128)(2,1)S(1)}, u32[]{:S(2)}, u32[]{:S(2)}) collective-permute-start(bf16[16,2048]{1,0:T(8,128)(2,1)S(1)} %add_convert_fusion.rest_0_), channel_id=1, source_target_pairs={{0,16},{4,20},{8,24},{12,28},{16,0},{20,4},{24,8},{28,12},{1,17},{... | collective-permute-start | bytes 196616 | tf_op jit(solution)/shard_map/ppermute | solution.py:315
  172.3 7.4 %collective-permute-done.21.rest_5_ = bf16[16,2048]{1,0:T(8,128)(2,1)S(1)} collective-permute-done((bf16[16,2048]{1,0:T(8,128)(2,1)S(1)}, bf16[16,2048]{1,0:T(8,128)(2,1)S(1)}, u32[]{:S(2)}, u32[]{:S(2)}) %collective-permute-start.21) | collective-permute-done | bytes 65568 | tf_op jit(solution)/shard_map/ppermute | solution.py:315
  179.7 6.7 %collective-permute-done.22.rest_6_ = bf16[16,2048]{1,0:T(8,128)(2,1)S(1)} collective-permute-done((bf16[16,2048]{1,0:T(8,128)(2,1)S(1)}, bf16[16,2048]{1,0:T(8,128)(2,1)S(1)}, u32[]{:S(2)}, u32[]{:S(2)}) %collective-permute-start.22) | collective-permute-done | bytes 65568 | tf_op jit(solution)/shard_map/ppermute | solution.py:315
  225.6 9.9 %stack.107.index_ref = s32[20]{0:T(128)S(1)} concatenate(s32[1]{0:T(128)} %bitcast, s32[1]{0:T(128)} %bitcast, s32[1]{0:T(128)} %bitcast, s32[1]{0:T(128)} %bitcast, s32[1]{0:T(128)} %get-tuple-element.96, s32[1]{0:T(128)} %get-tuple-element.95, s32[1]{0:T(128)} %get-tuple-element.96, s32[1]{0:T(128)} %get-tuple-element.95, s32[1]{0:T(128)} %get-tuple-element.94, ...), dimensions={0} | concatenate | bytes 160 | tf_op jit(solution)/shard_map/stack | solution.py:371
  247.2 7.2 %copies.4 = (bf16[4096,512]{1,0:T(8,128)(2,1)}, bf16[4096,512]{1,0:T(8,128)(2,1)}, bf16[2048,1024]{1,0:T(8,128)(2,1)}) custom-call(s32[20]{0:T(128)S(1)} %stack.107.index_ref, bf16[128,2048]{1,0:T(8,128)(2,1)} %copy-done.5, bf16[4096,256]{1,0:T(8,128)(2,1)} %get-tuple-element.62.bqv_ref, bf16[2048,128]{1,0:T(8,128)(2,1)} %copy-done.3, ...), custom_call_target="tpu_custom_call" | custom-call | tf_op jit(solution)/shard_map/copies/pallas_call | solution.py:288
  (245 shorter events, 111.9 us)
Async XLA Ops:
  26.9 22.9 %collective-permute-start.7 = (bf16[8,320,128]{2,1,0:T(8,128)(2,1)S(1)}, bf16[8,320,128]{2,1,0:T(8,128)(2,1)}, u32[]{:S(2)}, u32[]{:S(2)}) collective-permute-start(bf16[8,320,128]{2,1,0:T(8,128)(2,1)S(1)} %bitcast_dynamic-update-slice_fusion.rest_0_), channel_id=1, source_target_pairs={{0,2},{1,3},{2,0},{3,1},{4,6},{5,7},{6,4},{7,5},{8,10},{9,11},{10,... | collective-permute-start | bytes 1966088 | tf_op jit(solution)/shard_map/ppermute | solution.py:315
  28.4 24.0 %collective-permute-start.8 = (bf16[8,320,128]{2,1,0:T(8,128)(2,1)S(1)}, bf16[8,320,128]{2,1,0:T(8,128)(2,1)S(1)}, u32[]{:S(2)}, u32[]{:S(2)}) collective-permute-start(bf16[8,320,128]{2,1,0:T(8,128)(2,1)S(1)} %bitcast_dynamic-update-slice_fusion.rest_0_), channel_id=1, source_target_pairs={{0,1},{1,0},{2,3},{3,2},{4,5},{5,4},{6,7},{7,6},{8,9},{9,8},{10,11... | collective-permute-start | bytes 1966088 | tf_op jit(solution)/shard_map/ppermute | solution.py:315
  30.5 18.4 %collective-permute-start.48 = (bf16[384,512]{1,0:T(8,128)(2,1)S(1)}, bf16[384,512]{1,0:T(8,128)(2,1)S(1)}, u32[]{:S(2)}, u32[]{:S(2)}) collective-permute-start(bf16[384,512]{1,0:T(8,128)(2,1)S(1)} %get-tuple-element.71.rest_7_), channel_id=1, source_target_pairs={{8,0},{16,8},{24,16},{28,24},{20,28},{12,20},{4,12},{0,4},{9,1},{1... | collective-permute-start | bytes 1179656 | tf_op jit(solution)/shard_map/ppermute | solution.py:352
  53.3 29.5 %collective-permute-start.29 = (bf16[384,512]{1,0:T(8,128)(2,1)}, bf16[384,512]{1,0:T(8,128)(2,1)}, u32[]{:S(2)}, u32[]{:S(2)}) collective-permute-start(bf16[384,512]{1,0:T(8,128)(2,1)} %collective-permute-done.28.rest_12_), channel_id=1, source_target_pairs={{0,8},{8,16},{16,24},{24,28},{28,20},{20,12},{12,4},{4,0},{1,9},{9... | collective-permute-start | bytes 1179656 | tf_op jit(solution)/shard_map/ppermute | solution.py:352
  57.4 27.9 %collective-permute-start.36 = (bf16[384,512]{1,0:T(8,128)(2,1)}, bf16[384,512]{1,0:T(8,128)(2,1)}, u32[]{:S(2)}, u32[]{:S(2)}) collective-permute-start(bf16[384,512]{1,0:T(8,128)(2,1)} %collective-permute-done.35.rest_13_), channel_id=1, source_target_pairs={{8,0},{16,8},{24,16},{28,24},{20,28},{12,20},{4,12},{0,4},{9,1},{1... | collective-permute-start | bytes 1179656 | tf_op jit(solution)/shard_map/ppermute | solution.py:352
  61.0 24.4 %collective-permute-start.43 = (bf16[384,512]{1,0:T(8,128)(2,1)}, bf16[384,512]{1,0:T(8,128)(2,1)}, u32[]{:S(2)}, u32[]{:S(2)}) collective-permute-start(bf16[384,512]{1,0:T(8,128)(2,1)} %collective-permute-done.42.rest_14_), channel_id=1, source_target_pairs={{0,8},{8,16},{16,24},{24,28},{28,20},{20,12},{12,4},{4,0},{1,9},{9... | collective-permute-start | bytes 1179656 | tf_op jit(solution)/shard_map/ppermute | solution.py:352
  65.8 21.5 %collective-permute-start.50 = (bf16[384,512]{1,0:T(8,128)(2,1)}, bf16[384,512]{1,0:T(8,128)(2,1)}, u32[]{:S(2)}, u32[]{:S(2)}) collective-permute-start(bf16[384,512]{1,0:T(8,128)(2,1)} %collective-permute-done.49.rest_15_), channel_id=1, source_target_pairs={{8,0},{16,8},{24,16},{28,24},{20,28},{12,20},{4,12},{0,4},{9,1},{1... | collective-permute-start | bytes 1179656 | tf_op jit(solution)/shard_map/ppermute | solution.py:352
  85.3 41.2 %collective-permute-start.30 = (bf16[384,512]{1,0:T(8,128)(2,1)}, bf16[384,512]{1,0:T(8,128)(2,1)S(1)}, u32[]{:S(2)}, u32[]{:S(2)}) collective-permute-start(bf16[384,512]{1,0:T(8,128)(2,1)} %collective-permute-done.29.rest_16_), channel_id=1, source_target_pairs={{0,8},{8,16},{16,24},{24,28},{28,20},{20,12},{12,4},{4,0},{1,9},{9... | collective-permute-start | bytes 1179656 | tf_op jit(solution)/shard_map/ppermute | solution.py:352
  85.4 41.1 %collective-permute-start.37 = (bf16[384,512]{1,0:T(8,128)(2,1)}, bf16[384,512]{1,0:T(8,128)(2,1)S(1)}, u32[]{:S(2)}, u32[]{:S(2)}) collective-permute-start(bf16[384,512]{1,0:T(8,128)(2,1)} %collective-permute-done.36.rest_17_), channel_id=1, source_target_pairs={{8,0},{16,8},{24,16},{28,24},{20,28},{12,20},{4,12},{0,4},{9,1},{1... | collective-permute-start | bytes 1179656 | tf_op jit(solution)/shard_map/ppermute | solution.py:352
  87.4 41.8 %collective-permute-start.44 = (bf16[384,512]{1,0:T(8,128)(2,1)}, bf16[384,512]{1,0:T(8,128)(2,1)S(1)}, u32[]{:S(2)}, u32[]{:S(2)}) collective-permute-start(bf16[384,512]{1,0:T(8,128)(2,1)} %collective-permute-done.43.rest_18_), channel_id=1, source_target_pairs={{0,8},{8,16},{16,24},{24,28},{28,20},{20,12},{12,4},{4,0},{1,9},{9... | collective-permute-start | bytes 1179656 | tf_op jit(solution)/shard_map/ppermute | solution.py:352
  87.4 41.7 %collective-permute-start.51 = (bf16[384,512]{1,0:T(8,128)(2,1)}, bf16[384,512]{1,0:T(8,128)(2,1)S(1)}, u32[]{:S(2)}, u32[]{:S(2)}) collective-permute-start(bf16[384,512]{1,0:T(8,128)(2,1)} %collective-permute-done.50.rest_19_), channel_id=1, source_target_pairs={{8,0},{16,8},{24,16},{28,24},{20,28},{12,20},{4,12},{0,4},{9,1},{1... | collective-permute-start | bytes 1179656 | tf_op jit(solution)/shard_map/ppermute | solution.py:352
  89.4 16.6 %collective-permute-start.12 = (bf16[16,2048]{1,0:T(8,128)(2,1)S(1)}, bf16[16,2048]{1,0:T(8,128)(2,1)S(1)}, u32[]{:S(2)}, u32[]{:S(2)}) collective-permute-start(bf16[16,2048]{1,0:T(8,128)(2,1)S(1)} %get-tuple-element.54), channel_id=1, source_target_pairs={{0,12},{4,8},{8,4},{12,0},{16,28},{20,24},{24,20},{28,16},{1,13},{... | collective-permute-start | bytes 196616 | tf_op jit(solution)/shard_map/ppermute | solution.py:315
  129.1 18.8 %collective-permute-start.45 = (bf16[384,512]{1,0:T(8,128)(2,1)S(1)}, bf16[384,512]{1,0:T(8,128)(2,1)S(1)}, u32[]{:S(2)}, u32[]{:S(2)}) collective-permute-start(bf16[384,512]{1,0:T(8,128)(2,1)S(1)} %collective-permute-done.44.rest_22_), channel_id=1, source_target_pairs={{0,8},{8,16},{16,24},{24,28},{28,20},{20,12},{12,4},{4,0},{1,9},{9... | collective-permute-start | bytes 1179656 | tf_op jit(solution)/shard_map/ppermute | solution.py:352
  129.2 19.9 %collective-permute-start.52 = (bf16[384,512]{1,0:T(8,128)(2,1)S(1)}, bf16[384,512]{1,0:T(8,128)(2,1)S(1)}, u32[]{:S(2)}, u32[]{:S(2)}) collective-permute-start(bf16[384,512]{1,0:T(8,128)(2,1)S(1)} %collective-permute-done.51.rest_23_), channel_id=1, source_target_pairs={{8,0},{16,8},{24,16},{28,24},{20,28},{12,20},{4,12},{0,4},{9,1},{1... | collective-permute-start | bytes 1179656 | tf_op jit(solution)/shard_map/ppermute | solution.py:352
  131.6 19.8 %collective-permute-start.17 = (bf16[16,2048]{1,0:T(8,128)(2,1)S(1)}, bf16[16,2048]{1,0:T(8,128)(2,1)S(1)}, u32[]{:S(2)}, u32[]{:S(2)}) collective-permute-start(bf16[16,2048]{1,0:T(8,128)(2,1)S(1)} %add_convert_fusion.rest_0_), channel_id=1, source_target_pairs={{0,4},{4,0},{8,12},{12,8},{16,20},{20,16},{24,28},{28,24},{1,5},{5... | collective-permute-start | bytes 196616 | tf_op jit(solution)/shard_map/ppermute | solution.py:315
  139.5 49.0 %collective-permute-start.32 = (bf16[384,512]{1,0:T(8,128)(2,1)S(1)}, bf16[384,512]{1,0:T(8,128)(2,1)}, u32[]{:S(2)}, u32[]{:S(2)}) collective-permute-start(bf16[384,512]{1,0:T(8,128)(2,1)S(1)} %collective-permute-done.31.rest_4_), channel_id=1, source_target_pairs={{0,8},{8,16},{16,24},{24,28},{28,20},{20,12},{12,4},{4,0},{1,9},{9... | collective-permute-start | bytes 1179656 | tf_op jit(solution)/shard_map/ppermute | solution.py:352
  140.7 47.8 %collective-permute-start.39 = (bf16[384,512]{1,0:T(8,128)(2,1)S(1)}, bf16[384,512]{1,0:T(8,128)(2,1)}, u32[]{:S(2)}, u32[]{:S(2)}) collective-permute-start(bf16[384,512]{1,0:T(8,128)(2,1)S(1)} %collective-permute-done.38.rest_5_), channel_id=1, source_target_pairs={{8,0},{16,8},{24,16},{28,24},{20,28},{12,20},{4,12},{0,4},{9,1},{1... | collective-permute-start | bytes 1179656 | tf_op jit(solution)/shard_map/ppermute | solution.py:352
  147.9 42.6 %collective-permute-start.46 = (bf16[384,512]{1,0:T(8,128)(2,1)S(1)}, bf16[384,512]{1,0:T(8,128)(2,1)}, u32[]{:S(2)}, u32[]{:S(2)}) collective-permute-start(bf16[384,512]{1,0:T(8,128)(2,1)S(1)} %collective-permute-done.45.rest_6_), channel_id=1, source_target_pairs={{0,8},{8,16},{16,24},{24,28},{28,20},{20,12},{12,4},{4,0},{1,9},{9... | collective-permute-start | bytes 1179656 | tf_op jit(solution)/shard_map/ppermute | solution.py:352
  149.1 41.5 %collective-permute-start.53 = (bf16[384,512]{1,0:T(8,128)(2,1)S(1)}, bf16[384,512]{1,0:T(8,128)(2,1)}, u32[]{:S(2)}, u32[]{:S(2)}) collective-permute-start(bf16[384,512]{1,0:T(8,128)(2,1)S(1)} %collective-permute-done.52.rest_7_), channel_id=1, source_target_pairs={{8,0},{16,8},{24,16},{28,24},{20,28},{12,20},{4,12},{0,4},{9,1},{1... | collective-permute-start | bytes 1179656 | tf_op jit(solution)/shard_map/ppermute | solution.py:352
  186.5 16.9 %collective-permute-start.23 = (bf16[16,2048]{1,0:T(8,128)(2,1)S(1)}, bf16[16,2048]{1,0:T(8,128)(2,1)S(1)}, u32[]{:S(2)}, u32[]{:S(2)}) collective-permute-start(bf16[16,2048]{1,0:T(8,128)(2,1)S(1)} %add_convert_fusion.rest_0_), channel_id=1, source_target_pairs={{0,28},{4,24},{8,20},{12,16},{16,12},{20,8},{24,4},{28,0},{1,29},{... | collective-permute-start | bytes 196616 | tf_op jit(solution)/shard_map/ppermute | solution.py:315
  188.5 72.9 %collective-permute-start.33 = (bf16[384,512]{1,0:T(8,128)(2,1)}, bf16[384,512]{1,0:T(8,128)(2,1)}, u32[]{:S(2)}, u32[]{:S(2)}) collective-permute-start(bf16[384,512]{1,0:T(8,128)(2,1)} %collective-permute-done.32.rest_4_), channel_id=1, source_target_pairs={{0,8},{8,16},{16,24},{24,28},{28,20},{20,12},{12,4},{4,0},{1,9},{9... | collective-permute-start | bytes 1179656 | tf_op jit(solution)/shard_map/ppermute | solution.py:352
  188.5 72.9 %collective-permute-start.40 = (bf16[384,512]{1,0:T(8,128)(2,1)}, bf16[384,512]{1,0:T(8,128)(2,1)}, u32[]{:S(2)}, u32[]{:S(2)}) collective-permute-start(bf16[384,512]{1,0:T(8,128)(2,1)} %collective-permute-done.39.rest_5_), channel_id=1, source_target_pairs={{8,0},{16,8},{24,16},{28,24},{20,28},{12,20},{4,12},{0,4},{9,1},{1... | collective-permute-start | bytes 1179656 | tf_op jit(solution)/shard_map/ppermute | solution.py:352
  190.5 70.9 %collective-permute-start.47 = (bf16[384,512]{1,0:T(8,128)(2,1)}, bf16[384,512]{1,0:T(8,128)(2,1)}, u32[]{:S(2)}, u32[]{:S(2)}) collective-permute-start(bf16[384,512]{1,0:T(8,128)(2,1)} %collective-permute-done.46.rest_6_), channel_id=1, source_target_pairs={{0,8},{8,16},{16,24},{24,28},{28,20},{20,12},{12,4},{4,0},{1,9},{9... | collective-permute-start | bytes 1179656 | tf_op jit(solution)/shard_map/ppermute | solution.py:352
  190.6 70.8 %collective-permute-start.54 = (bf16[384,512]{1,0:T(8,128)(2,1)}, bf16[384,512]{1,0:T(8,128)(2,1)}, u32[]{:S(2)}, u32[]{:S(2)}) collective-permute-start(bf16[384,512]{1,0:T(8,128)(2,1)} %collective-permute-done.53.rest_7_), channel_id=1, source_target_pairs={{8,0},{16,8},{24,16},{28,24},{20,28},{12,20},{4,12},{0,4},{9,1},{1... | collective-permute-start | bytes 1179656 | tf_op jit(solution)/shard_map/ppermute | solution.py:352
  (97 other events, 1595.3 us)
